TPU v7x, 32 devices: a whole 2x2x4 slice. The times are simulated.
32 devices in a mesh: sp: 8 (over z, y), dp: 4 (over x, core).
Axes of the slice: x: 2, y: 2, z: 4, core: 2. Of those that a mesh axis runs over, the one named last changes fastest.
Arguments:
- query_nope: bfloat16 [4, 2048, 16, 128], P('dp', 'sp'), may hold values from -6 to 6
- query_rope: bfloat16 [4, 2048, 16, 64], P('dp', 'sp'), may hold values from -160 to 160
- latent: bfloat16 [4, 2048, 256], P('dp', 'sp'), may hold values from -6 to 6
- key_rope: bfloat16 [4, 2048, 64], P('dp', 'sp'), may hold values from -4 to 4
- resid: bfloat16 [4, 2048, 2048], P('dp', 'sp'), may hold values from -6 to 6
- latent_gain: float32 [256], replicated, may hold values from 0.1 to 1.9
- key_up: bfloat16 [256, 2048], P(None, 'sp'), may hold values from -0.375 to 0.375
- value_up: bfloat16 [256, 2048], P(None, 'sp'), may hold values from -0.375 to 0.375
- out_proj: bfloat16 [2048, 2048], P('sp', 'dp'), may hold values from -0.125 to 0.125
- norm_gain: float32 [2048], replicated, may hold values from 0.1 to 1.9
- expert_gate: bfloat16 [8, 2048, 1024], P('sp'), may hold values from -0.125 to 0.125
- expert_up: bfloat16 [8, 2048, 1024], P('sp'), may hold values from -0.125 to 0.125
- expert_down: bfloat16 [8, 1024, 2048], P('sp'), may hold values from -0.1875 to 0.1875
- routes: int32 [4, 2048, 2], P('dp', 'sp'), may hold values from 0 to 7, all different within a row; in each aligned block of 256 rows (0 to 255, 256 to 511, ..., all dimensions but the last counted through in order) at most 128 rows name the same one
- route_weight: float32 [4, 2048, 2], P('dp', 'sp'), may hold values from 0.2 to 1
Outputs:
- mixed: bfloat16 [4, 2048, 2048], P('dp', 'sp')
Inputs may be any that keep to these rules, and one draw needn't show every extreme that they name: `routes`: each token names two different experts. Among the tokens of one device no expert is named more than 128 times, and in every draw some expert is named exactly 128 times by some device's tokens.
All inputs are finite; a program needn't handle non-finite values.
Results may differ from a plain program's by a relative error of at most 0.0075.
Values may be sent and summed in bfloat16 or wider, within the bound.
A program may use at most 128 MiB of HBM per device.

v0:
```python
import jax
import jax.numpy as jnp
from jax import lax
from jax.sharding import PartitionSpec as P

epsilon = 1e-06
rope_base = 10000.0
masked_score = -1e30


def rotate(values, positions):
    half_width = values.shape[-1] // 2
    frequency = rope_base ** (-jnp.arange(half_width, dtype=jnp.float32) / half_width)
    angles = positions.astype(jnp.float32)[:, None] * frequency[None, :]
    cosine = jnp.cos(angles)
    sine_part = jnp.sin(angles)
    if values.ndim == 3:
        cosine = cosine[:, None, :]
        sine_part = sine_part[:, None, :]
    floats = values.astype(jnp.float32)
    first_half = floats[..., :half_width]
    second_half = floats[..., half_width:]
    turned = jnp.concatenate(
        [
            first_half * cosine - second_half * sine_part,
            second_half * cosine + first_half * sine_part,
        ],
        axis=-1,
    )
    return turned.astype(jnp.bfloat16)


def rms_scaled(values, gain):
    floats = values.astype(jnp.float32)
    return floats * lax.rsqrt(jnp.mean(floats * floats, axis=-1, keepdims=True) + epsilon) * gain


def assign_slots(route_block, experts_all, capacity):
    flat_routes = route_block.reshape(-1)
    onehot = (flat_routes[:, None] == jnp.arange(experts_all, dtype=jnp.int32)[None, :]).astype(
        jnp.int32
    )
    earlier = jnp.cumsum(onehot, axis=0) - onehot
    placed = jnp.sum(earlier * onehot, axis=1)
    return flat_routes * capacity + placed


def fill_slots(rows, slot_ids, experts_all, capacity):
    pairs = slot_ids.shape[0]
    matches = jnp.arange(experts_all * capacity, dtype=jnp.int32)[:, None] == slot_ids[None, :]
    source = (
        jnp.sum(jnp.where(matches, jnp.arange(pairs, dtype=jnp.int32)[None, :], 0), axis=1) // 2
    )
    filled = jnp.any(matches, axis=1)
    picked = jnp.take(rows, source, axis=0)
    chosen = jnp.where(filled[:, None], picked, jnp.zeros_like(picked))
    return chosen.reshape(experts_all, capacity, rows.shape[-1])


def combine_slots(returned, slot_ids, weights):
    flat_back = returned.reshape(-1, returned.shape[-1])
    picked = (
        jnp.take(flat_back, slot_ids, axis=0).astype(jnp.float32).reshape(weights.shape[0], 2, -1)
    )
    return jnp.sum(weights[:, :, None] * picked, axis=1)


def shards(
    query_nope,
    query_rope,
    latent,
    key_rope,
    resid,
    latent_gain,
    key_up,
    value_up,
    out_proj,
    norm_gain,
    expert_gate,
    expert_up,
    expert_down,
    routes,
    route_weight,
):
    tokens_here = latent.shape[1]
    sp_count = lax.axis_size("sp")
    length = tokens_here * sp_count
    block = min(512, length)
    blocks = length // block
    local_pos = lax.axis_index("sp") * tokens_here + jnp.arange(tokens_here, dtype=jnp.int32)
    latent_normed = rms_scaled(latent[0], latent_gain).astype(jnp.bfloat16)
    key_turned = rotate(key_rope[0], local_pos)
    query_turned = rotate(query_rope[0], local_pos)
    all_latent, all_keyturn = (
        lax.all_gather(latent_normed, "sp", axis=0, tiled=True),
        lax.all_gather(key_turned, "sp", axis=0, tiled=True),
    )
    query_plain, query_turn = (
        lax.all_to_all(query_nope[0], "sp", split_axis=1, concat_axis=0, tiled=True),
        lax.all_to_all(query_turned, "sp", split_axis=1, concat_axis=0, tiled=True),
    )
    heads_here = query_plain.shape[1]
    key_plain = (
        jnp.dot(all_latent, key_up, preferred_element_type=jnp.float32)
        .astype(jnp.bfloat16)
        .reshape(length, heads_here, -1)
    )
    value_heads = (
        jnp.dot(all_latent, value_up, preferred_element_type=jnp.float32)
        .astype(jnp.bfloat16)
        .reshape(length, heads_here, -1)
    )
    scale = (query_plain.shape[-1] + query_turn.shape[-1]) ** (-0.5)
    key_ids = jnp.arange(length, dtype=jnp.int32)

    def one_block(items):
        index, plain_block, turn_block = items
        scores = jnp.einsum(
            "bhd,shd->hbs", plain_block, key_plain, preferred_element_type=jnp.float32
        )
        scores = (
            scores
            + jnp.einsum("bhr,sr->hbs", turn_block, all_keyturn, preferred_element_type=jnp.float32)
        ) * scale
        row_ids = index * block + jnp.arange(block, dtype=jnp.int32)
        allowed = key_ids[None, :] <= row_ids[:, None]
        scores = jnp.where(allowed[None], scores, masked_score)
        largest = jnp.max(scores, axis=-1, keepdims=True)
        powers = jnp.exp(scores - largest)
        attend = (powers / jnp.sum(powers, axis=-1, keepdims=True)).astype(jnp.bfloat16)
        return jnp.einsum(
            "hbs,shd->bhd", attend, value_heads, preferred_element_type=jnp.float32
        ).astype(jnp.bfloat16)

    attended = lax.map(
        one_block,
        (
            jnp.arange(blocks, dtype=jnp.int32),
            query_plain.reshape(blocks, block, heads_here, -1),
            query_turn.reshape(blocks, block, heads_here, -1),
        ),
    )
    attended = attended.reshape(length, heads_here, -1)
    token_heads = lax.all_to_all(attended, "sp", split_axis=0, concat_axis=1, tiled=True)
    flat_heads = token_heads.reshape(tokens_here, -1)
    head_rows = lax.all_gather(out_proj, "dp", axis=1, tiled=True)
    projected = jnp.dot(
        flat_heads,
        lax.all_gather(head_rows, "sp", axis=0, tiled=True),
        preferred_element_type=jnp.float32,
    ).astype(jnp.bfloat16)
    after_attention = resid[0].astype(jnp.float32) + projected.astype(jnp.float32)
    normed = rms_scaled(after_attention, norm_gain).astype(jnp.bfloat16)
    experts_all = sp_count * expert_gate.shape[0]
    capacity = 4 * tokens_here // experts_all
    slot_ids = assign_slots(routes[0], experts_all, capacity)
    outgoing = fill_slots(normed, slot_ids, experts_all, capacity)
    arrived = lax.all_to_all(outgoing, "sp", split_axis=0, concat_axis=0, tiled=True)
    senders, slots_now, width = arrived.shape
    rows = arrived.reshape(senders * slots_now, width)
    gate = jnp.dot(rows, expert_gate[0], preferred_element_type=jnp.float32)
    upward = jnp.dot(rows, expert_up[0], preferred_element_type=jnp.float32)
    hidden = (jax.nn.silu(gate) * upward).astype(jnp.bfloat16)
    result = jnp.dot(hidden, expert_down[0], preferred_element_type=jnp.float32).astype(
        jnp.bfloat16
    )
    returned = lax.all_to_all(
        result.reshape(senders, slots_now, width), "sp", split_axis=0, concat_axis=0, tiled=True
    )
    routed = combine_slots(returned, slot_ids, route_weight[0])
    return (after_attention + routed).astype(jnp.bfloat16)[None]


def solution(mesh):
    return jax.shard_map(
        shards,
        mesh=mesh,
        in_specs=(
            P("dp", "sp", None, None),
            P("dp", "sp", None, None),
            P("dp", "sp", None),
            P("dp", "sp", None),
            P("dp", "sp", None),
            P(),
            P(None, "sp"),
            P(None, "sp"),
            P("sp", "dp"),
            P(),
            P("sp", None, None),
            P("sp", None, None),
            P("sp", None, None),
            P("dp", "sp", None),
            P("dp", "sp", None),
        ),
        out_specs=P("dp", "sp", None),
        check_vma=False,
    )
```

profile of v0, /device:TPU:0, one launch (start us, length us, event | category | flops | bytes accessed | tf_op | source)
XLA Modules:
  0.0 489.6 jit_solution(9054582442500225814)
XLA Ops:
  12.2 16.1 %all-gather.6.cloned.1.call-done = bf16[256,2048]{1,0:T(8,128)(2,1)} async-done(((bf16[256,512]{1,0:T(8,128)(2,1)}), bf16[256,2048]{1,0:T(8,128)(2,1)}) %all-gather.6.cloned.1.call-update) | async-done | bytes 1048592 | tf_op jit(solution)/shard_map/all_gather | solution.py:146
  29.4 5.5 %all-to-all-start.1 = ((bf16[256,16,64]{0,2,1:T(8,128)(2,1)}), bf16[256,16,64]{0,2,1:T(8,128)(2,1)S(1)}, u32[]{:S(2)}, u32[]{:S(2)}) async-start(bf16[256,16,64]{0,2,1:T(8,128)(2,1)} %pad_maximum_fusion), calls=%async_computation.1 | async-start | bytes 1048576 | tf_op jit(solution)/shard_map/all_to_all | solution.py:100
  36.2 17.7 %all-to-all-done.1 = bf16[256,16,64]{0,2,1:T(8,128)(2,1)S(1)} async-done(((bf16[256,16,64]{0,2,1:T(8,128)(2,1)}), bf16[256,16,64]{0,2,1:T(8,128)(2,1)S(1)}, u32[]{:S(2)}, u32[]{:S(2)}) %all-to-all-start.1) | async-done | bytes 524320 | tf_op jit(solution)/shard_map/all_to_all | solution.py:100
  54.0 3.6 all-to-all-start
  57.6 55.9 %all_gather.13 = bf16[2048,64]{0,1:T(8,128)(2,1)S(1)} all-gather(bf16[256,64]{0,1:T(8,128)(2,1)S(1)} %pad_maximum_fusion.1), channel_id=1, replica_groups=mesh['sp'=8,'dp'=4] {'sp'}, dimensions={0}, use_global_device_ids=true | all-gather | bytes 294912 | tf_op jit(solution)/shard_map/all_gather | solution.py:96
  124.3 73.1 %while.11 = (s32[]{:T(128)}, bf16[4,512,2,128]{3,1,0,2:T(8,128)(2,1)}, s32[4]{0:T(128)S(1)}, bf16[4,512,2,128]{3,1,0,2:T(8,128)(2,1)S(1)}, bf16[2048,2,128]{2,0,...) while((s32[]{:T(128)}, ...), condition=%wide.region_4.5_spmd.clone, body=%wide.region_1.4_spmd.clone.sunk | while | flops 1360139776 | bytes 93205688 | solution.py:135
  133.3 9.1 %fusion.77 = bf16[4,512,2,128]{3,1,0,2:T(8,128)(2,1)} fusion(bf16[4,512,2,128]{3,1,0,2:T(8,128)(2,1)} %get-tuple-element.211, s32[]{:T(128)} %get-tuple-element.210, bf16[2048,2,128]{2,0,1:T(8,128)(2,1)S(1)} %copy-done.5, f32[2,512]{1,0:T(2,128)S(1)} %fusion.76, f32[2,512,2048]{2,1,0:T(8,128)} %copy-done.2), kind=kOutput, calls=%fused_computation.13.clone.1 | convolution fusion | flops 543296512 | bytes 18092544 | tf_op jit(solution)/shard_map/while/body/eval_jaxpr/hbs,shd->bhd/dot_general | solution.py:131
  151.5 9.2 %fusion.77 = bf16[4,512,2,128]{3,1,0,2:T(8,128)(2,1)} fusion(bf16[4,512,2,128]{3,1,0,2:T(8,128)(2,1)} %get-tuple-element.211, s32[]{:T(128)} %get-tuple-element.210, bf16[2048,2,128]{2,0,1:T(8,128)(2,1)S(1)} %copy-done.5, f32[2,512]{1,0:T(2,128)S(1)} %fusion.76, f32[2,512,2048]{2,1,0:T(8,128)} %copy-done.2), kind=kOutput, calls=%fused_computation.13.clone.1 | convolution fusion | flops 543296512 | bytes 18092544 | tf_op jit(solution)/shard_map/while/body/eval_jaxpr/hbs,shd->bhd/dot_general | solution.py:131
  169.8 9.1 %fusion.77 = bf16[4,512,2,128]{3,1,0,2:T(8,128)(2,1)} fusion(bf16[4,512,2,128]{3,1,0,2:T(8,128)(2,1)} %get-tuple-element.211, s32[]{:T(128)} %get-tuple-element.210, bf16[2048,2,128]{2,0,1:T(8,128)(2,1)S(1)} %copy-done.5, f32[2,512]{1,0:T(2,128)S(1)} %fusion.76, f32[2,512,2048]{2,1,0:T(8,128)} %copy-done.2), kind=kOutput, calls=%fused_computation.13.clone.1 | convolution fusion | flops 543296512 | bytes 18092544 | tf_op jit(solution)/shard_map/while/body/eval_jaxpr/hbs,shd->bhd/dot_general | solution.py:131
  188.0 9.4 %fusion.77 = bf16[4,512,2,128]{3,1,0,2:T(8,128)(2,1)} fusion(bf16[4,512,2,128]{3,1,0,2:T(8,128)(2,1)} %get-tuple-element.211, s32[]{:T(128)} %get-tuple-element.210, bf16[2048,2,128]{2,0,1:T(8,128)(2,1)S(1)} %copy-done.5, f32[2,512]{1,0:T(2,128)S(1)} %fusion.76, f32[2,512,2048]{2,1,0:T(8,128)} %copy-done.2), kind=kOutput, calls=%fused_computation.13.clone.1 | convolution fusion | flops 543296512 | bytes 18092544 | tf_op jit(solution)/shard_map/while/body/eval_jaxpr/hbs,shd->bhd/dot_general | solution.py:131
  197.3 3.7 copy.95
  201.0 3.7 all-to-all-start.2
  207.4 28.0 %all-to-all-done.2 = bf16[2048,2,128]{2,1,0:T(2,128)(2,1)S(1)} async-done(((bf16[2048,2,128]{2,1,0:T(2,128)(2,1)}), bf16[2048,2,128]{2,1,0:T(2,128)(2,1)S(1)}, u32[]{:S(2)}, u32[]{:S(2)}) %all-to-all-start.2) | async-done | bytes 1048608 | tf_op jit(solution)/shard_map/all_to_all | solution.py:144
  236.2 6.1 %multiply_reduce_fusion.1 = (f32[256]{0:T(256)S(1)}, f32[256,2048]{1,0:T(8,128)S(1)}) fusion(bf16[256,2048]{0,1:T(8,128)(2,1)S(1)} %bitcast.150, bf16[2048,2048]{1,0:T(8,128)(2,1)} %all-gather.8.cloned.1.call-done, bf16[1,256,2048]{2,1,0:T(8,128)(2,1)} %param.21), kind=kOutput, calls=%fused_computation.42 | convolution fusion | flops 2150629120 | bytes 12583936 | tf_op jit(solution)/shard_map/dot_general | solution.py:147
  242.5 6.0 %gather_fusion = bf16[1024,2048]{1,0:T(8,128)(2,1)} fusion(bf16[256,2048]{1,0:T(8,128)(2,1)S(1)} %multiply_convert_fusion.1, s32[1024]{0:T(1024)S(1)} %broadcast_clamp_fusion), kind=kCustom, calls=%fused_computation | custom fusion | bytes 8392704 | tf_op jit(solution)/shard_map/jit(_take)/gather | solution.py:55
  251.1 95.5 %all_to_all.55 = bf16[8,128,2048]{2,1,0:T(8,128)(2,1)S(1)} all-to-all(bf16[8,128,2048]{2,1,0:T(8,128)(2,1)S(1)} %select_select_fusion), channel_id=1, replica_groups=mesh['sp'=8,'dp'=4] {'sp'}, dimensions={0} | all-to-all | bytes 8388608 | tf_op jit(solution)/shard_map/all_to_all | solution.py:158
  346.6 4.5 fusion.20
  351.1 5.4 %multiply_convert_fusion = bf16[1024,1024]{1,0:T(8,128)(2,1)S(1)} fusion(f32[1024,1024]{1,0:T(8,128)S(1)} %fusion.20, bf16[1024,2048]{1,0:T(8,128)(2,1)S(1)} %bitcast.154, bf16[1,2048,1024]{2,1,0:T(8,128)(2,1)S(1)} %copy-done.10), kind=kOutput, calls=%fused_computation.31 | convolution fusion | flops 4301258752 | bytes 14680064 | tf_op jit(solution)/shard_map/dot_general | solution.py:161
  356.5 6.1 %fusion.24 = bf16[1024,2048]{1,0:T(8,128)(2,1)} fusion(bf16[1024,1024]{1,0:T(8,128)(2,1)S(1)} %multiply_convert_fusion, bf16[1,1024,2048]{2,1,0:T(8,128)(2,1)S(1)} %copy-done.11), kind=kOutput, calls=%fused_computation.34 | convolution fusion | flops 4297064448 | bytes 10485760 | tf_op jit(solution)/shard_map/dot_general | solution.py:164
  362.6 4.9 all-to-all-start.4
  368.4 91.0 %all-to-all-done.4 = bf16[8,128,2048]{2,1,0:T(8,128)(2,1)} async-done(((bf16[8,128,2048]{2,1,0:T(8,128)(2,1)}), bf16[8,128,2048]{2,1,0:T(8,128)(2,1)}, u32[]{:S(2)}, u32[]{:S(2)}) %all-to-all-start.4) | async-done | bytes 4194336 | tf_op jit(solution)/shard_map/all_to_all | solution.py:167
  459.4 8.0 %gather_fusion.1 = bf16[512,2048]{1,0:T(8,128)(2,1)} fusion(bf16[1024,2048]{1,0:T(8,128)(2,1)} %bitcast.33, s32[1024]{0:T(1024)S(1)} %pad_clamp_fusion), kind=kCustom, calls=%fused_computation.1 | custom fusion | bytes 4196352 | tf_op jit(solution)/shard_map/jit(_take)/gather | solution.py:63
  467.4 4.4 gather.15
  471.9 9.9 %multiply_reduce_fusion = f32[256,2048]{1,0:T(8,128)S(1)} fusion(bf16[256,2,2048]{2,1,0:T(2,128)(2,1)} %gather.15, pred[256,2]{1,0:T(8,128)(4,1)S(1)} %copy.102, f32[256,2]{1,0:T(8,128)S(1)} %copy.98), kind=kLoop, calls=%fused_computation.30 | loop fusion | flops 3670016 | bytes 4196864 | tf_op jit(solution)/shard_map/reduce_sum | solution.py:65
  (122 shorter events, 60.6 us)
Async XLA Ops:
  6.5 108.5 %copy-start = (bf16[256,256]{1,0:T(8,128)(2,1)S(1)}, bf16[256,256]{1,0:T(8,128)(2,1)}, u32[]{:S(2)}) copy-start(bf16[256,256]{1,0:T(8,128)(2,1)} %param.23) | copy-start | bytes 393220
  6.5 28.3 %copy-start.4 = (bf16[1,256,16,128]{3,2,1,0:T(8,128)(2,1)S(1)}, bf16[1,256,16,128]{3,2,1,0:T(8,128)(2,1)}, u32[]{:S(2)}) copy-start(bf16[1,256,16,128]{3,2,1,0:T(8,128)(2,1)} %param.17) | copy-start | bytes 3145732
  6.5 21.8 %all-gather.6.cloned.1.call-start = ((), (), s32[]{:S(2)}) async-start(), calls=%async_computation.6 | async-start | bytes 1310720 | tf_op jit(solution)/shard_map/all_gather | solution.py:146
  7.3 107.8 %all-gather.4.cloned.1.call-start = ((), (), s32[]{:S(2)}) async-start(), calls=%async_computation.5 | async-start | bytes 1179648 | tf_op jit(solution)/shard_map/all_gather | solution.py:95
  10.0 226.1 %all-gather.8.cloned.1.call-start = ((), (), s32[]{:S(2)}) async-start(), calls=%async_computation.7 | async-start | bytes 9437184 | tf_op jit(solution)/shard_map/all_gather | solution.py:149
  29.4 24.6 %all-to-all-start.1 = ((bf16[256,16,64]{0,2,1:T(8,128)(2,1)}), bf16[256,16,64]{0,2,1:T(8,128)(2,1)S(1)}, u32[]{:S(2)}, u32[]{:S(2)}) async-start(bf16[256,16,64]{0,2,1:T(8,128)(2,1)} %pad_maximum_fusion), calls=%async_computation.1 | async-start | bytes 1048576 | tf_op jit(solution)/shard_map/all_to_all | solution.py:100
  54.0 70.2 %all-to-all-start = ((bf16[256,16,128]{2,0,1:T(8,128)(2,1)}), bf16[256,16,128]{2,0,1:T(8,128)(2,1)S(1)}, u32[]{:S(2)}, u32[]{:S(2)}) async-start(bf16[256,16,128]{2,0,1:T(8,128)(2,1)} %bitcast.127), calls=%async_computation | async-start | bytes 2097152 | tf_op jit(solution)/shard_map/all_to_all | solution.py:99
  115.1 4.4 copy-start.3
  130.1 3.2 copy-start.2
  130.1 3.2 copy-start.5
  148.3 3.2 copy-start.2
  148.3 3.2 copy-start.5
  166.5 3.2 copy-start.2
  184.7 3.2 copy-start.2
  184.7 3.2 copy-start.5
  197.3 7.4 %copy-start.6 = (s32[1,256,2]{1,2,0:T(2,128)S(1)}, s32[1,256,2]{1,2,0:T(2,128)}, u32[]{:S(2)}) copy-start(s32[1,256,2]{1,2,0:T(2,128)} %param.30) | copy-start | bytes 6148
  201.0 34.4 %all-to-all-start.2 = ((bf16[2048,2,128]{2,1,0:T(2,128)(2,1)}), bf16[2048,2,128]{2,1,0:T(2,128)(2,1)S(1)}, u32[]{:S(2)}, u32[]{:S(2)}) async-start(bf16[2048,2,128]{2,1,0:T(2,128)(2,1)} %copy.95), calls=%async_computation.2 | async-start | bytes 2097152 | tf_op jit(solution)/shard_map/all_to_all | solution.py:144
  236.1 6.1 %copy-start.7 = (f32[2048]{0:T(1024)S(1)}, f32[2048]{0:T(1024)}, u32[]{:S(2)}) copy-start(f32[2048]{0:T(1024)} %param.26) | copy-start | bytes 24580
  251.1 95.5 %copy-start.9 = (bf16[1,2048,1024]{2,1,0:T(8,128)(2,1)S(1)}, bf16[1,2048,1024]{2,1,0:T(8,128)(2,1)}, u32[]{:S(2)}) copy-start(bf16[1,2048,1024]{2,1,0:T(8,128)(2,1)} %param.28) | copy-start | bytes 12582916
  346.6 4.5 copy-start.10
  351.1 5.4 %copy-start.11 = (bf16[1,1024,2048]{2,1,0:T(8,128)(2,1)S(1)}, bf16[1,1024,2048]{2,1,0:T(8,128)(2,1)}, u32[]{:S(2)}) copy-start(bf16[1,1024,2048]{2,1,0:T(8,128)(2,1)} %param.29) | copy-start | bytes 12582916
  362.6 5.6 %copy-start.8 = (f32[1,256,2]{1,2,0:T(2,128)S(1)}, f32[1,256,2]{1,2,0:T(2,128)}, u32[]{:S(2)}) copy-start(f32[1,256,2]{1,2,0:T(2,128)} %param.31) | copy-start | bytes 6148
  362.6 96.9 %all-to-all-start.4 = ((bf16[8,128,2048]{2,1,0:T(8,128)(2,1)}), bf16[8,128,2048]{2,1,0:T(8,128)(2,1)}, u32[]{:S(2)}, u32[]{:S(2)}) async-start(bf16[8,128,2048]{2,1,0:T(8,128)(2,1)} %bitcast.152), calls=%async_computation.4 | async-start | bytes 8388608 | tf_op jit(solution)/shard_map/all_to_all | solution.py:167
  467.4 15.6 %copy-start.1 = (bf16[256,256]{1,0:T(8,128)(2,1)S(1)}, bf16[256,256]{1,0:T(8,128)(2,1)}, u32[]{:S(2)}) copy-start(bf16[256,256]{1,0:T(8,128)(2,1)} %param.23) | copy-start | bytes 393220
  (1 other events, 3.2 us)
Sparse Core Ops, SparseCore 0:
  8.9 19.4 all-gather.5
  30.5 57.7 all-gather.3
  90.4 131.3 all-gather.7
where the time goes:
time: 490 us
  waiting for transfers between devices  154 us (31%)
  blocking collectives  151 us (31%)
  matrix products  80.1 us (16%)
  local copies, waits for them, and re-layouts  40 us (8%)
  other arithmetic  30.5 us (6%)
  starting transfers between devices  17.9 us (4%)
  between operations  13.5 us (3%)
    all_to_all x1, blocking collectives, shards(): lax.all_to_all(outgoing, 'sp', split_axis=0, concat_axis=0, tiled=True)  95.5 us
    all_to_all x1, waiting for transfers between devices, shards(): lax.all_to_all(result.reshape(senders, slots_now, width), 'sp', split_axi...  91 us
    all_gather x1, blocking collectives, shards(): lax.all_gather(key_turned, 'sp', axis=0, tiled=True)  55.9 us
    dot_general x4, matrix products, one_block(): jnp.einsum('hbs,shd->bhd', attend, value_heads, preferred_element_type=jn...  36.8 us
    all_to_all x1, waiting for transfers between devices, shards(): lax.all_to_all(attended, 'sp', split_axis=0, concat_axis=1, tiled=True)  28 us
    all_to_all x1, waiting for transfers between devices, shards(): lax.all_to_all(query_turned, 'sp', split_axis=1, concat_axis=0, tiled=True)  17.7 us
    all_gather x1, waiting for transfers between devices, shards(): head_rows = lax.all_gather(out_proj, 'dp', axis=1, tiled=True)  16.1 us
    gather x2, local copies, waits for them, and re-layouts, combine_slots(): jnp.take(flat_back, slot_ids, axis=0).astype(jnp.float32)  12.4 us
  transfers between devices with their start and end apart: 7, of which 4 were waited for; matrix products, arithmetic and copies ran while one was open for 18% of the time, Pallas kernels for 0%

commit v1 on v0

v1 whole, which is shorter than its diff:
```python
import functools

import jax
import jax.numpy as jnp
from jax import lax
from jax.experimental import pallas as pl
from jax.experimental.pallas import tpu as pltpu
from jax.sharding import PartitionSpec as P

epsilon = 1e-06
rope_base = 10000.0
masked_score = -1e30
log2_e = 1.4426950408889634


def rotate(values, positions):
    half_width = values.shape[-1] // 2
    frequency = rope_base ** (-jnp.arange(half_width, dtype=jnp.float32) / half_width)
    angles = positions.astype(jnp.float32)[:, None] * frequency[None, :]
    cosine = jnp.cos(angles)
    sine_part = jnp.sin(angles)
    if values.ndim == 3:
        cosine = cosine[:, None, :]
        sine_part = sine_part[:, None, :]
    floats = values.astype(jnp.float32)
    first_half = floats[..., :half_width]
    second_half = floats[..., half_width:]
    turned = jnp.concatenate(
        [
            first_half * cosine - second_half * sine_part,
            second_half * cosine + first_half * sine_part,
        ],
        axis=-1,
    )
    return turned.astype(jnp.bfloat16)


def rms_scaled(values, gain):
    floats = values.astype(jnp.float32)
    return floats * lax.rsqrt(jnp.mean(floats * floats, axis=-1, keepdims=True) + epsilon) * gain


def attend_kernel(heads_here, nope, channels, scale, me_ref, query_ref, shared_ref, ups_ref, out_ref):
    group = pl.program_id(0)
    columns = heads_here * nope
    me = me_ref[0]
    tokens = shared_ref.shape[1]
    ups = ups_ref[0].reshape(channels, 2 * columns)
    up_keys = ups[:, 0:columns]
    up_values = ups[:, columns : 2 * columns]
    up_values_t = jnp.transpose(up_values.astype(jnp.float32)).astype(jnp.bfloat16)

    def scores_of(chunk):
        latent = shared_ref[chunk, :, 0:channels]
        turned = shared_ref[chunk, :, channels:]
        keys = jnp.dot(latent, up_keys, preferred_element_type=jnp.float32).astype(jnp.bfloat16)
        values_t = lax.dot_general(
            up_values_t, latent, (((1,), (1,)), ((), ())), preferred_element_type=jnp.float32
        ).astype(jnp.bfloat16)
        scores = []
        for head in range(heads_here):
            full = jnp.concatenate([keys[:, head * nope : (head + 1) * nope], turned], axis=1)
            scores.append(
                jnp.dot(full, query_ref[head], preferred_element_type=jnp.float32)
                * (scale * log2_e)
            )
        return scores, [values_t[h * nope : (h + 1) * nope, :] for h in range(heads_here)]

    key_ids = lax.broadcasted_iota(jnp.int32, (tokens, tokens), 0)
    query_ids = lax.broadcasted_iota(jnp.int32, (tokens, tokens), 1)
    allowed = key_ids <= query_ids
    scores, values = scores_of(me)
    state = []
    for score, value in zip(scores, values):
        score = jnp.where(allowed, score, masked_score)
        largest = jnp.max(score, axis=0, keepdims=True)
        powers = jnp.exp2(score - largest)
        state.append(
            (
                largest,
                jnp.sum(powers, axis=0, keepdims=True),
                jnp.dot(value, powers.astype(jnp.bfloat16), preferred_element_type=jnp.float32),
            )
        )

    def step(chunk, state):
        scores, values = scores_of(chunk)
        after = []
        for (largest, total, kept), score, value in zip(state, scores, values):
            now = jnp.maximum(largest, jnp.max(score, axis=0, keepdims=True))
            fade = jnp.exp2(largest - now)
            powers = jnp.exp2(score - now)
            after.append(
                (
                    now,
                    total * fade + jnp.sum(powers, axis=0, keepdims=True),
                    kept * fade
                    + jnp.dot(
                        value, powers.astype(jnp.bfloat16), preferred_element_type=jnp.float32
                    ),
                )
            )
        return tuple(after)

    state = lax.fori_loop(0, me, step, tuple(state))
    for head, (_, total, kept) in enumerate(state):
        out_ref[:, head * nope : (head + 1) * nope] = jnp.transpose(kept / total).astype(
            out_ref.dtype
        )


def attend(me, queries_t, shared, ups, heads_here, nope, channels, scale):
    groups, tokens, width = shared.shape
    columns = heads_here * nope
    depth = queries_t.shape[1]
    return pl.pallas_call(
        functools.partial(attend_kernel, heads_here, nope, channels, scale),
        grid_spec=pltpu.PrefetchScalarGridSpec(
            num_scalar_prefetch=1,
            grid=(groups,),
            in_specs=[
                pl.BlockSpec((heads_here, depth, tokens), lambda g, me: (g, 0, 0)),
                pl.BlockSpec((groups, tokens, width), lambda g, me: (0, 0, 0)),
                pl.BlockSpec((1,) + ups.shape[1:], lambda g, me: (g, 0, 0, 0)),
            ],
            out_specs=pl.BlockSpec((tokens, columns), lambda g, me: (0, g)),
        ),
        out_shape=jax.ShapeDtypeStruct((tokens, groups * columns), jnp.bfloat16),
        cost_estimate=pl.CostEstimate(
            flops=20 * groups * tokens * groups * tokens * columns,
            bytes_accessed=2 * groups * tokens * width,
            transcendentals=0,
        ),
    )(me, queries_t, shared, ups)


def project_kernel(heads_ref, weight_ref, resid_ref, gain_ref, after_ref, normed_ref, square_ref):
    part = pl.program_id(0)
    rows, width = weight_ref.shape[0] * weight_ref.shape[2], weight_ref.shape[3]
    weight = weight_ref[...].reshape(rows, width)
    projected = (
        jnp.dot(heads_ref[...], weight, preferred_element_type=jnp.float32)
        .astype(jnp.bfloat16)
        .astype(jnp.float32)
    )
    after = resid_ref[...].astype(jnp.float32) + projected
    after_ref[part] = after

    @pl.when(part == 0)
    def _():
        square_ref[...] = jnp.zeros_like(square_ref)

    square_ref[...] += jnp.sum(after * after, axis=1, keepdims=True)

    @pl.when(part == pl.num_programs(0) - 1)
    def _():
        parts = after_ref.shape[0]
        factor = lax.rsqrt(square_ref[...] / (parts * width) + epsilon)
        for at in range(parts):
            cols = slice(at * width, (at + 1) * width)
            normed_ref[:, cols] = (after_ref[at] * factor * gain_ref[:, cols]).astype(
                normed_ref.dtype
            )


def project(heads, weights, resid, gain):
    groups, parts, rows, width = weights.shape
    tokens = heads.shape[0]
    return pl.pallas_call(
        project_kernel,
        grid=(parts,),
        in_specs=[
            pl.BlockSpec((tokens, groups * rows), lambda p: (0, 0)),
            pl.BlockSpec((groups, 1, rows, width), lambda p: (0, p, 0, 0)),
            pl.BlockSpec((tokens, width), lambda p: (0, p)),
            pl.BlockSpec((1, parts * width), lambda p: (0, 0)),
        ],
        out_specs=[
            pl.BlockSpec((parts, tokens, width), lambda p: (0, 0, 0)),
            pl.BlockSpec((tokens, parts * width), lambda p: (0, 0)),
        ],
        out_shape=[
            jax.ShapeDtypeStruct((parts, tokens, width), jnp.float32),
            jax.ShapeDtypeStruct((tokens, parts * width), jnp.bfloat16),
        ],
        scratch_shapes=[pltpu.VMEM((tokens, 1), jnp.float32)],
        cost_estimate=pl.CostEstimate(
            flops=2 * tokens * groups * rows * parts * width,
            bytes_accessed=2 * groups * rows * parts * width,
            transcendentals=0,
        ),
    )(heads, weights, resid, gain)


def in_three(values):
    high = lax.reduce_precision(values, 8, 7)
    middle = lax.reduce_precision(values - high, 8, 7)
    low = values - high - middle
    return [piece.astype(jnp.bfloat16) for piece in (high, middle, low)]


def shards(
    query_nope,
    query_rope,
    latent,
    key_rope,
    resid,
    latent_gain,
    key_up,
    value_up,
    out_proj,
    norm_gain,
    expert_gate,
    expert_up,
    expert_down,
    routes,
    route_weight,
):
    tokens, channels = latent.shape[1:]
    sp_count = lax.axis_size("sp")
    dp_count = lax.axis_size("dp")
    me = lax.axis_index("sp")
    nope, rope = query_nope.shape[-1], query_rope.shape[-1]
    heads_here = key_up.shape[1] // nope
    scale = (nope + rope) ** (-0.5)
    local_pos = me * tokens + jnp.arange(tokens, dtype=jnp.int32)
    latent_normed = rms_scaled(latent[0], latent_gain).astype(jnp.bfloat16)
    key_turned = rotate(key_rope[0], local_pos)
    spare = 128 - rope
    shared = lax.all_gather(
        jnp.concatenate(
            [latent_normed, key_turned, jnp.zeros((tokens, spare), jnp.bfloat16)],
            axis=1,
        ),
        "sp",
        axis=0,
    )
    piece = channels // dp_count
    ups = lax.dynamic_slice_in_dim(
        jnp.concatenate([key_up, value_up], axis=1), lax.axis_index("dp") * piece, piece, axis=0
    )
    ups = lax.all_gather(ups, ("sp", "dp"), axis=0).reshape(sp_count, dp_count, piece, -1)
    weights = lax.all_gather(out_proj, ("sp", "dp"), axis=0)
    weights = weights.reshape(sp_count, dp_count, *out_proj.shape)
    query_turned = rotate(query_rope[0], local_pos)
    queries = jnp.concatenate(
        [query_nope[0], query_turned, jnp.zeros(query_turned.shape[:2] + (128 - rope,), jnp.bfloat16)],
        axis=-1,
    )
    queries_t = jnp.transpose(queries, (1, 2, 0))
    heads = attend(
        me.astype(jnp.int32)[None], queries_t, shared, ups, heads_here, nope, channels, scale
    )
    after, normed = project(heads, weights, resid[0], norm_gain[None])

    experts_all = sp_count * expert_gate.shape[0]
    capacity = 4 * tokens // experts_all
    ids = jnp.arange(experts_all, dtype=jnp.int32)[:, None, None]
    mine = routes[0][None] == ids
    named = jnp.any(mine, axis=-1)
    weight = jnp.sum(jnp.where(mine, route_weight[0][None], 0.0), axis=-1)
    place = jnp.cumsum(named.astype(jnp.int32), axis=1) - 1
    chosen = (
        place[:, None, :] == jnp.arange(capacity, dtype=jnp.int32)[None, :, None]
    ) & named[:, None, :]
    select = chosen.astype(jnp.bfloat16).reshape(experts_all * capacity, tokens)
    outgoing = jnp.dot(select, normed, preferred_element_type=jnp.float32).astype(jnp.bfloat16)
    rows = lax.all_to_all(outgoing, "sp", split_axis=0, concat_axis=0, tiled=True)
    gate = jnp.dot(rows, expert_gate[0], preferred_element_type=jnp.float32)
    upward = jnp.dot(rows, expert_up[0], preferred_element_type=jnp.float32)
    hidden = (jax.nn.silu(gate) * upward).astype(jnp.bfloat16)
    result = jnp.dot(hidden, expert_down[0], preferred_element_type=jnp.float32).astype(
        jnp.bfloat16
    )
    returned = lax.all_to_all(result, "sp", split_axis=0, concat_axis=0, tiled=True)
    mixing = jnp.where(chosen, weight[:, None, :], 0.0).reshape(experts_all * capacity, tokens)
    routed = sum(
        lax.dot_general(part, returned, (((0,), (0,)), ((), ())), preferred_element_type=jnp.float32)
        for part in in_three(mixing)[0:2]
    )
    after = jnp.concatenate([after[p] for p in range(dp_count)], axis=1)
    return (after + routed).astype(jnp.bfloat16)[None]


def solution(mesh):
    return jax.shard_map(
        shards,
        mesh=mesh,
        in_specs=(
            P("dp", "sp", None, None),
            P("dp", "sp", None, None),
            P("dp", "sp", None),
            P("dp", "sp", None),
            P("dp", "sp", None),
            P(),
            P(None, "sp"),
            P(None, "sp"),
            P("sp", "dp"),
            P(),
            P("sp", None, None),
            P("sp", None, None),
            P("sp", None, None),
            P("dp", "sp", None),
            P("dp", "sp", None),
        ),
        out_specs=P("dp", "sp", None),
        check_vma=False,
    )
```

time: 490 us -> 431 us (0.88)
  waiting for transfers between devices: 154 us -> 259 us
  matrix products: 80.1 us -> 26.4 us
  blocking collectives: 151 us -> 97.7 us
  local copies, waits for them, and re-layouts: 40 us -> 3.55 us
  other arithmetic: 30.5 us -> 8.42 us
  Pallas kernels: 0 us -> 17.3 us
  starting transfers between devices: 17.9 us -> 4.77 us
    all_gather x3, waiting for transfers between devices: 16.1 us -> 167 us  [the longest x1 69.8 us: shards(): weights = lax.all_gather(out_proj, ('sp', 'dp'), axis=0)]
    all_gather x1 -> x0, blocking collectives: 55.9 us -> none  [shards(): lax.all_gather(key_turned, 'sp', axis=0, tiled=True)]
    dot_general x15 -> x3, matrix products: 64.1 us -> 10.5 us  [the longest x2 8 us: shards(): lax.dot_general(part, returned, (((0,), (0,)), ((), ())), preferred_eleme...]
    all_to_all x4 -> x1, waiting for transfers between devices: 137 us -> 91.1 us  [shards(): lax.all_to_all(result, 'sp', split_axis=0, concat_axis=0, tiled=True)]
    gather x3 -> x0, local copies, waits for them, and re-layouts: 18.5 us -> none  [the longest x2 12.4 us: combine_slots(): jnp.take(flat_back, slot_ids, axis=0).astype(jnp.float32)]
    pallas_call x0 -> x2, Pallas kernels: none -> 17.3 us  [the longest x1 9.05 us: attend(): pl.pallas_call(functools.partial(attend_kernel, heads_here, nope, channel...]
    all_to_all x4 -> x1, starting transfers between devices: 17.8 us -> 4.68 us  [shards(): lax.all_to_all(result, 'sp', split_axis=0, concat_axis=0, tiled=True)]
    reduce_sum x3 -> x1, other arithmetic: 10.3 us -> 0.01 us  [shards(): weight = jnp.sum(jnp.where(mine, route_weight[0][None], 0.0), axis=-1)]
  transfers between devices with their start and end apart: 7 -> 4, of which waited for: 4 -> 4; matrix products, arithmetic and copies ran while one was open for 18% -> 2% of each run, Pallas kernels for 0% -> 2%
where the time goes in v1:
time: 431 us; the launch traced here: 430 us
  waiting for transfers between devices  259 us (60%)
  blocking collectives  97.7 us (23%)
  matrix products  26.4 us (6%)
  Pallas kernels  17.3 us (4%)
  between operations  13.3 us (3%)
  other arithmetic  8.42 us (2%)
  starting transfers between devices  4.77 us (1%)
    all_to_all x1, blocking collectives, shards(): lax.all_to_all(outgoing, 'sp', split_axis=0, concat_axis=0, tiled=True)  97.7 us
    all_to_all x1, waiting for transfers between devices, shards(): lax.all_to_all(result, 'sp', split_axis=0, concat_axis=0, tiled=True)  91.1 us
    all_gather x1, waiting for transfers between devices, shards(): weights = lax.all_gather(out_proj, ('sp', 'dp'), axis=0)  69.8 us
    all_gather x1, waiting for transfers between devices, shards(): lax.all_gather(ups, ('sp', 'dp'), axis=0)  57.4 us
    all_gather x1, waiting for transfers between devices, shards(): lax.all_gather(jnp.concatenate([latent_normed, key_turned, jnp.zeros((tok...  39.7 us
    pallas_call x1, Pallas kernels, attend(): pl.pallas_call(functools.partial(attend_kernel, heads_here, nope, channel...  9.05 us
  transfers between devices with their start and end apart: 4, of which 4 were waited for; matrix products, arithmetic and copies ran while one was open for 2% of the time, Pallas kernels for 2%

profile of v1, /device:TPU:0, one launch (start us, length us, event | category | flops | bytes accessed | tf_op | source)
XLA Modules:
  0.0 430.3 jit_solution(14771340767762232271)
XLA Ops:
  6.6 0.8 bitcast_convert_fusion.1
  7.8 1.0 fusion.28
  9.0 1.0 fusion.30
  10.0 0.8 maximum_maximum_fusion
  10.8 1.4 fusion.31
  12.3 0.7 all-gather.11.cloned.1.call-update
  13.1 1.6 copy.28
  14.8 0.6 reduce-window.6
  16.2 1.9 maximum_bitcast_fusion.query_ref
  18.2 39.7 %all-gather.7.cloned.1.call-done = bf16[2048,384]{1,0:T(8,128)(2,1)} async-done(((bf16[256,384]{1,0:T(8,128)(2,1)}), bf16[2048,384]{1,0:T(8,128)(2,1)}) %all-gather.7.cloned.1.call-update) | async-done | bytes 1572880 | tf_op jit(solution)/shard_map/all_gather | solution.py:230
  57.8 57.4 %all-gather.9.cloned.1.call-done = bf16[2048,512]{1,0:T(8,128)(2,1)} async-done(((bf16[64,512]{1,0:T(8,128)(2,1)}), bf16[2048,512]{1,0:T(8,128)(2,1)}) %all-gather.9.cloned.1.call-update) | async-done | bytes 2097168 | tf_op jit(solution)/shard_map/all_gather | solution.py:242
  115.3 9.0 %shard_map.145.heads_ref = bf16[256,2048]{1,0:T(8,128)(2,1)} custom-call(s32[1]{0:T(128)} %bitcast.me_ref, bf16[16,256,256]{2,1,0:T(8,128)(2,1)} %maximum_bitcast_fusion.query_ref, bf16[8,256,384]{2,1,0:T(8,128)(2,1)} %bitcast.90, bf16[8,4,64,512]{3,2,1,0:T(8,128)(2,1)} %bitcast.89), custom_call_target="tpu_custom_call" | custom-call | flops 21474836480 | bytes 1572864 | tf_op jit(solution)/shard_map/pallas_call | solution.py:116
  124.3 69.8 %all-gather.11.cloned.1.call-done = bf16[8192,512]{1,0:T(8,128)(2,1)} async-done(((bf16[256,512]{1,0:T(8,128)(2,1)}), bf16[8192,512]{1,0:T(8,128)(2,1)}) %all-gather.11.cloned.1.call-update) | async-done | bytes 8388624 | tf_op jit(solution)/shard_map/all_gather | solution.py:243
  194.1 8.2 %shard_map.146 = (f32[4,256,512]{2,1,0:T(8,128)}, bf16[256,2048]{1,0:T(8,128)(2,1)}) custom-call(bf16[256,2048]{1,0:T(8,128)(2,1)} %shard_map.145.heads_ref, bf16[8,4,256,512]{3,2,1,0:T(8,128)(2,1)} %bitcast.79, bf16[256,2048]{1,0:T(8,128)(2,1)} %bitcast.84, f32[1,2048]{1,0:T(1,128)} %bitcast.87), custom_call_target="tpu_custom_call" | custom-call | flops 2147483648 | bytes 8388608 | tf_op jit(solution)/shard_map/pallas_call | solution.py:169
  202.4 2.5 convolution_convert_fusion
  204.9 97.7 %all_to_all.21 = bf16[8,128,2048]{2,1,0:T(8,128)(2,1)S(1)} all-to-all(bf16[8,128,2048]{2,1,0:T(8,128)(2,1)S(1)} %bitcast.78), channel_id=1, replica_groups=mesh['sp'=8,'dp'=4] {'sp'}, dimensions={0} | all-to-all | bytes 8388608 | tf_op jit(solution)/shard_map/all_to_all | solution.py:268
  302.6 4.5 %fusion.2 = f32[1024,1024]{1,0:T(8,128)S(1)} fusion(bf16[1024,2048]{1,0:T(8,128)(2,1)S(1)} %bitcast.81, bf16[1,2048,1024]{2,1,0:T(8,128)(2,1)S(1)} %copy-done.6), kind=kOutput, calls=%fused_computation.2 | convolution fusion | flops 4294967296 | bytes 12582912 | tf_op jit(solution)/shard_map/dot_general | solution.py:270
  307.1 5.4 %multiply_convert_fusion = bf16[1024,1024]{1,0:T(8,128)(2,1)S(1)} fusion(f32[1024,1024]{1,0:T(8,128)S(1)} %fusion.2, bf16[1024,2048]{1,0:T(8,128)(2,1)S(1)} %bitcast.82, bf16[1,2048,1024]{2,1,0:T(8,128)(2,1)S(1)} %copy-done.7), kind=kOutput, calls=%fused_computation.6 | convolution fusion | flops 4301258752 | bytes 14680064 | tf_op jit(solution)/shard_map/dot_general | solution.py:269
  312.5 6.1 %fusion.6 = bf16[1024,2048]{1,0:T(8,128)(2,1)} fusion(bf16[1024,1024]{1,0:T(8,128)(2,1)S(1)} %multiply_convert_fusion, bf16[1,1024,2048]{2,1,0:T(8,128)(2,1)S(1)} %copy-done.8), kind=kOutput, calls=%fused_computation.8 | convolution fusion | flops 4297064448 | bytes 10485760 | tf_op jit(solution)/shard_map/dot_general | solution.py:272
  318.6 4.7 %all-to-all-start.1 = ((bf16[8,128,2048]{2,1,0:T(8,128)(2,1)}), bf16[8,128,2048]{2,1,0:T(8,128)(2,1)}, u32[]{:S(2)}, u32[]{:S(2)}) async-start(bf16[8,128,2048]{2,1,0:T(8,128)(2,1)} %bitcast.80), calls=%async_computation.1 | async-start | bytes 8388608 | tf_op jit(solution)/shard_map/all_to_all | solution.py:275
  323.3 1.3 slice_bitcast_fusion.3
  324.6 91.1 %all-to-all-done.1 = bf16[8,128,2048]{2,1,0:T(8,128)(2,1)} async-done(((bf16[8,128,2048]{2,1,0:T(8,128)(2,1)}), bf16[8,128,2048]{2,1,0:T(8,128)(2,1)}, u32[]{:S(2)}, u32[]{:S(2)}) %all-to-all-start.1) | async-done | bytes 4194336 | tf_op jit(solution)/shard_map/all_to_all | solution.py:275
  415.7 3.5 convolution_bitcast_fusion
  419.3 4.5 %fusion.14 = bf16[1,256,2048]{2,1,0:T(8,128)(2,1)} fusion(f32[256,2048]{1,0:T(8,128)S(1)} %convolution_bitcast_fusion, bf16[8,128,2048]{2,1,0:T(8,128)(2,1)} %all-to-all-done.1, f32[256,512]{1,0:T(8,128)S(1)} %get-tuple-element.10, f32[256,512]{1,0:T(8,128)S(1)} %copy-done.1, f32[256,512]{1,0:T(8,128)S(1)} %copy-done.2, ...), kind=kOutput, calls=%fused_computation.14 | convolution fusion | flops 1078198272 | bytes 9455616 | tf_op jit(solution)/shard_map/dot_general | solution.py:278
  (43 shorter events, 1.6 us)
Async XLA Ops:
  6.5 8.2 %copy-start.4 = (s32[1,256,2]{1,2,0:T(2,128)S(1)}, s32[1,256,2]{1,2,0:T(2,128)}, u32[]{:S(2)}) copy-start(s32[1,256,2]{1,2,0:T(2,128)} %param.28) | copy-start | bytes 6148
  6.5 9.4 %copy-start.3 = (bf16[1,256,16,64]{1,3,2,0:T(8,128)(2,1)S(1)}, bf16[1,256,16,64]{1,3,2,0:T(8,128)(2,1)}, u32[]{:S(2)}) copy-start(bf16[1,256,16,64]{1,3,2,0:T(8,128)(2,1)} %param.16) | copy-start | bytes 1572868
  6.5 51.3 %all-gather.7.cloned.1.call-start = ((), (), s32[]{:S(2)}) async-start(), calls=%async_computation.2 | async-start | bytes 1769472 | tf_op jit(solution)/shard_map/all_gather | solution.py:230
  10.8 104.5 %all-gather.9.cloned.1.call-start = ((), (), s32[]{:S(2)}) async-start(), calls=%async_computation.3 | async-start | bytes 2162688 | tf_op jit(solution)/shard_map/all_gather | solution.py:242
  12.3 181.9 %all-gather.11.cloned.1.call-start = ((), (), s32[]{:S(2)}) async-start(), calls=%async_computation.4 | async-start | bytes 8650752 | tf_op jit(solution)/shard_map/all_gather | solution.py:243
  204.9 97.8 %copy-start.6 = (bf16[1,2048,1024]{2,1,0:T(8,128)(2,1)S(1)}, bf16[1,2048,1024]{2,1,0:T(8,128)(2,1)}, u32[]{:S(2)}) copy-start(bf16[1,2048,1024]{2,1,0:T(8,128)(2,1)} %param.26) | copy-start | bytes 12582916
  302.6 4.5 %copy-start.7 = (bf16[1,2048,1024]{2,1,0:T(8,128)(2,1)S(1)}, bf16[1,2048,1024]{2,1,0:T(8,128)(2,1)}, u32[]{:S(2)}) copy-start(bf16[1,2048,1024]{2,1,0:T(8,128)(2,1)} %param.25) | copy-start | bytes 12582916
  307.1 5.4 %copy-start.8 = (bf16[1,1024,2048]{2,1,0:T(8,128)(2,1)S(1)}, bf16[1,1024,2048]{2,1,0:T(8,128)(2,1)}, u32[]{:S(2)}) copy-start(bf16[1,1024,2048]{2,1,0:T(8,128)(2,1)} %param.27) | copy-start | bytes 12582916
  318.6 4.7 %copy-start.5 = (f32[1,256,2]{1,2,0:T(2,128)S(1)}, f32[1,256,2]{1,2,0:T(2,128)}, u32[]{:S(2)}) copy-start(f32[1,256,2]{1,2,0:T(2,128)} %param.29) | copy-start | bytes 6148
  318.6 4.7 %copy-start = (f32[4,256,512]{2,1,0:T(8,128)S(1)}, f32[4,256,512]{2,1,0:T(8,128)}, u32[]{:S(2)}) copy-start(f32[4,256,512]{2,1,0:T(8,128)} %get-tuple-element.7) | copy-start | bytes 6291460
  318.6 97.1 %all-to-all-start.1 = ((bf16[8,128,2048]{2,1,0:T(8,128)(2,1)}), bf16[8,128,2048]{2,1,0:T(8,128)(2,1)}, u32[]{:S(2)}, u32[]{:S(2)}) async-start(bf16[8,128,2048]{2,1,0:T(8,128)(2,1)} %bitcast.80), calls=%async_computation.1 | async-start | bytes 8388608 | tf_op jit(solution)/shard_map/all_to_all | solution.py:275
  324.6 94.7 %copy-start.1 = (f32[256,512]{1,0:T(8,128)S(1)}, f32[256,512]{1,0:T(8,128)}, u32[]{:S(2)}) copy-start(f32[256,512]{1,0:T(8,128)} %get-tuple-element.11) | copy-start | bytes 1572868
  324.6 94.7 %copy-start.2 = (f32[256,512]{1,0:T(8,128)S(1)}, f32[256,512]{1,0:T(8,128)}, u32[]{:S(2)}) copy-start(f32[256,512]{1,0:T(8,128)} %get-tuple-element.12) | copy-start | bytes 1572868
Sparse Core Ops, SparseCore 0:
  10.9 46.8 all-gather.6
  60.7 54.5 all-gather.8
  118.2 75.9 all-gather.10

commit v2 on v1

--- a/solution.py
+++ b/solution.py
@@ -1,4 +1,5 @@
 import functools
+import math
 
 import jax
 import jax.numpy as jnp
@@ -45,7 +46,7 @@
     columns = heads_here * nope
     me = me_ref[0]
     tokens = shared_ref.shape[1]
-    ups = ups_ref[0].reshape(channels, 2 * columns)
+    ups = ups_ref[...].reshape(channels, 2 * columns)
     up_keys = ups[:, 0:columns]
     up_values = ups[:, columns : 2 * columns]
     up_values_t = jnp.transpose(up_values.astype(jnp.float32)).astype(jnp.bfloat16)
@@ -121,7 +122,7 @@
             in_specs=[
                 pl.BlockSpec((heads_here, depth, tokens), lambda g, me: (g, 0, 0)),
                 pl.BlockSpec((groups, tokens, width), lambda g, me: (0, 0, 0)),
-                pl.BlockSpec((1,) + ups.shape[1:], lambda g, me: (g, 0, 0, 0)),
+                pl.BlockSpec((ups.shape[0], 1) + ups.shape[2:], lambda g, me: (0, g, 0, 0)),
             ],
             out_specs=pl.BlockSpec((tokens, columns), lambda g, me: (0, g)),
         ),
@@ -190,6 +191,117 @@
             transcendentals=0,
         ),
     )(heads, weights, resid, gain)
+
+
+def gather_kernel(
+    outer, inner, dp_count, row_ref, piece_ref, rows_ref, pieces_ref,
+    own_sems, far_send, far_recv, near_send, near_recv, dp_send, dp_recv,
+):
+    me = lax.axis_index("sp")
+    dp = lax.axis_index("dp")
+    far, near = me // inner, lax.rem(me, inner)
+    barrier = pltpu.get_barrier_semaphore()
+    fars = [lax.rem(far + step, outer) for step in range(1, outer)]
+    nears = [lax.rem(near + step, inner) for step in range(1, inner)]
+    dps = [lax.rem(dp + step, dp_count) for step in range(1, dp_count)]
+    greeted = (
+        [{"sp": f * inner + near} for f in fars]
+        + [{"sp": far * inner + n} for n in nears]
+        + [{"dp": d} for d in dps]
+    )
+    for peer in greeted:
+        pl.semaphore_signal(barrier, inc=1, device_id=peer, device_id_type=pl.DeviceIdType.MESH)
+    pl.semaphore_wait(barrier, len(greeted))
+
+    def remote(source, target, send, recv, peer):
+        copy = pltpu.make_async_remote_copy(
+            src_ref=source, dst_ref=target, send_sem=send, recv_sem=recv,
+            device_id=peer, device_id_type=pl.DeviceIdType.MESH,
+        )
+        copy.start()
+        return copy
+
+    def pair(row, piece, block, send, recv, peer):
+        return [
+            remote(row, rows_ref.at[block], send.at[0], recv.at[0], peer),
+            remote(piece, pieces_ref.at[dp, block], send.at[1], recv.at[1], peer),
+        ]
+
+    out_far = []
+    for at, f in enumerate(fars):
+        out_far.append(pair(row_ref, piece_ref, me, far_send.at[at], far_recv.at[at], {"sp": f * inner + near}))
+    last = []
+
+    def share(block):
+        for at, d in enumerate(dps):
+            last.append(
+                remote(
+                    pieces_ref.at[dp, block], pieces_ref.at[dp, block],
+                    dp_send.at[len(last)], dp_recv.at[len(last)], {"dp": d},
+                )
+            )
+
+    sends = []
+    for at, n in enumerate(nears):
+        sends.append(pair(row_ref, piece_ref, me, near_send.at[0, at], near_recv.at[0, at], {"sp": far * inner + n}))
+    own = [
+        pltpu.make_async_copy(row_ref, rows_ref.at[me], own_sems.at[0]),
+        pltpu.make_async_copy(piece_ref, pieces_ref.at[dp, me], own_sems.at[1]),
+    ]
+    for copy in own:
+        copy.start()
+    for copy in own:
+        copy.wait()
+    share(me)
+    for at in range(outer - 1):
+        for copy in out_far[at]:
+            copy.wait_recv()
+        block = lax.rem(far + outer - 1 - at, outer) * inner + near
+        for to, n in enumerate(nears):
+            sends.append(
+                pair(
+                    rows_ref.at[block], pieces_ref.at[dp, block], block,
+                    near_send.at[at + 1, to], near_recv.at[at + 1, to], {"sp": far * inner + n},
+                )
+            )
+        share(block)
+    for at in range(outer):
+        for to in range(inner - 1):
+            for copy in sends[at * (inner - 1) + to]:
+                copy.wait_recv()
+            column = lax.rem(near + inner - 1 - to, inner)
+            share(lax.rem(far + outer - at, outer) * inner + column)
+    for copies in out_far + sends:
+        for copy in copies:
+            copy.wait_send()
+    for copy in last:
+        copy.wait()
+
+
+def gather_shared(row, piece, sp_count, dp_count, number):
+    inner = max(d for d in range(1, math.isqrt(sp_count) + 1) if sp_count % d == 0)
+    outer = sp_count // inner
+    dma = pltpu.SemaphoreType.DMA
+    return pl.pallas_call(
+        functools.partial(gather_kernel, outer, inner, dp_count),
+        out_shape=[
+            jax.ShapeDtypeStruct((sp_count,) + row.shape, row.dtype),
+            jax.ShapeDtypeStruct((dp_count, sp_count) + piece.shape, piece.dtype),
+        ],
+        in_specs=[pl.BlockSpec(memory_space=pltpu.VMEM)] * 2,
+        out_specs=[pl.BlockSpec(memory_space=pltpu.VMEM)] * 2,
+        scratch_shapes=[
+            dma((2,)),
+            dma((max(outer - 1, 1), 2)),
+            dma((max(outer - 1, 1), 2)),
+            dma((outer, max(inner - 1, 1), 2)),
+            dma((outer, max(inner - 1, 1), 2)),
+            dma((max(dp_count - 1, 1) * sp_count,)),
+            dma((max(dp_count - 1, 1) * sp_count,)),
+        ],
+        compiler_params=pltpu.CompilerParams(collective_id=number, has_side_effects=True),
+        cost_estimate=pl.CostEstimate(flops=2 * 10**10, bytes_accessed=10**7, transcendentals=0),
+    )(row, piece)
 
 
 def in_three(values):
@@ -227,19 +339,14 @@
     latent_normed = rms_scaled(latent[0], latent_gain).astype(jnp.bfloat16)
     key_turned = rotate(key_rope[0], local_pos)
     spare = 128 - rope
-    shared = lax.all_gather(
-        jnp.concatenate(
-            [latent_normed, key_turned, jnp.zeros((tokens, spare), jnp.bfloat16)],
-            axis=1,
-        ),
-        "sp",
-        axis=0,
+    row = jnp.concatenate(
+        [latent_normed, key_turned, jnp.zeros((tokens, spare), jnp.bfloat16)], axis=1
     )
     piece = channels // dp_count
     ups = lax.dynamic_slice_in_dim(
         jnp.concatenate([key_up, value_up], axis=1), lax.axis_index("dp") * piece, piece, axis=0
     )
-    ups = lax.all_gather(ups, ("sp", "dp"), axis=0).reshape(sp_count, dp_count, piece, -1)
+    shared, ups = gather_shared(row, ups, sp_count, dp_count, 0)
     weights = lax.all_gather(out_proj, ("sp", "dp"), axis=0)
     weights = weights.reshape(sp_count, dp_count, *out_proj.shape)
     query_turned = rotate(query_rope[0], local_pos)

time: 431 us -> 362 us (0.84)
  waiting for transfers between devices: 259 us -> 120 us
  Pallas kernels: 17.3 us -> 74.5 us
  blocking collectives: 97.7 us -> 111 us
    all_gather x2 -> x0, waiting for transfers between devices: 97.1 us -> none  [the longest x1 57.4 us: shards(): lax.all_gather(ups, ('sp', 'dp'), axis=0)]
    pallas_call x0 -> x1, Pallas kernels: none -> 57 us  [gather_shared(): pl.pallas_call(functools.partial(gather_kernel, outer, inner, dp_count),...]
    all_gather x1, waiting for transfers between devices: 69.8 us -> 27.4 us  [shards(): weights = lax.all_gather(out_proj, ('sp', 'dp'), axis=0)]
    all_to_all x1, blocking collectives: 97.7 us -> 111 us  [shards(): lax.all_to_all(outgoing, 'sp', split_axis=0, concat_axis=0, tiled=True)]
  transfers between devices with their start and end apart: 4 -> 2, of which waited for: 4 -> 2; matrix products, arithmetic and copies ran while one was open for 2% -> 3% of each run, Pallas kernels for 2% -> 18%
where the time goes in v2:
time: 362 us; the launch traced here: 361 us
  waiting for transfers between devices  120 us (33%)
  blocking collectives  111 us (31%)
  Pallas kernels  74.5 us (21%)
  matrix products  26.4 us (7%)
  between operations  13.6 us (4%)
  other arithmetic  6.87 us (2%)
  starting transfers between devices  4.68 us (1%)
  local copies, waits for them, and re-layouts  4.33 us (1%)
    all_to_all x1, blocking collectives, shards(): lax.all_to_all(outgoing, 'sp', split_axis=0, concat_axis=0, tiled=True)  111 us
    all_to_all x1, waiting for transfers between devices, shards(): lax.all_to_all(result, 'sp', split_axis=0, concat_axis=0, tiled=True)  91.7 us
    pallas_call x1, Pallas kernels, gather_shared(): pl.pallas_call(functools.partial(gather_kernel, outer, inner, dp_count),...  57 us
    all_gather x1, waiting for transfers between devices, shards(): weights = lax.all_gather(out_proj, ('sp', 'dp'), axis=0)  27.4 us
    pallas_call x1, Pallas kernels, attend(): pl.pallas_call(functools.partial(attend_kernel, heads_here, nope, channel...  9.22 us
    pallas_call x1, Pallas kernels, project(): pl.pallas_call(project_kernel, grid=(parts,), in_specs=[pl.BlockSpec((tok...  8.24 us
    dot_general x2, matrix products, shards(): lax.dot_general(part, returned, (((0,), (0,)), ((), ())), preferred_eleme...  7.99 us
  transfers between devices with their start and end apart: 2, of which 2 were waited for; matrix products, arithmetic and copies ran while one was open for 3% of the time, Pallas kernels for 18%

profile of v2, /device:TPU:0, one launch (start us, length us, event | category | flops | bytes accessed | tf_op | source)
XLA Modules:
  0.0 361.5 jit_solution(12690636377496625040)
XLA Ops:
  6.5 0.7 all-gather.3.cloned.1.call-update
  7.4 0.9 copy.40
  8.4 0.6 subtract_convert_fusion.1
  9.1 1.6 copy.36
  10.7 0.7 fusion.32
  11.4 0.6 reduce-window.6
  12.3 0.3 fusion.18
  12.6 1.4 fusion.31.piece_ref
  14.3 0.8 maximum_maximum_fusion.row_ref
  15.3 2.0 maximum_bitcast_fusion.query_ref
  17.3 57.0 %shard_map.145 = (bf16[8,256,384]{2,1,0:T(8,128)(2,1)}, bf16[4,8,64,512]{3,2,1,0:T(8,128)(2,1)}) custom-call(bf16[256,384]{1,0:T(8,128)(2,1)} %maximum_maximum_fusion.row_ref, bf16[64,512]{1,0:T(8,128)(2,1)} %fusion.31.piece_ref), custom_call_target="tpu_custom_call" | custom-call | flops 20000000000 | bytes 10000000 | tf_op jit(solution)/shard_map/pallas_call | solution.py:285
  74.3 9.2 %shard_map.146.heads_ref = bf16[256,2048]{1,0:T(8,128)(2,1)} custom-call(s32[1]{0:T(128)} %bitcast.me_ref, bf16[16,256,256]{2,1,0:T(8,128)(2,1)} %maximum_bitcast_fusion.query_ref, bf16[8,256,384]{2,1,0:T(8,128)(2,1)} %get-tuple-element.9.shared_ref, bf16[4,8,64,512]{3,2,1,0:T(8,128)(2,1)} %get-tuple-element.10.ups_ref), custom_call_target="tpu_custom_call" | custom-call | flops 21474836480 | bytes 1572864 | tf_op jit(solution)/shard_map/pallas_call | solution.py:117
  83.5 27.4 %all-gather.3.cloned.1.call-done = bf16[8192,512]{1,0:T(8,128)(2,1)} async-done(((bf16[256,512]{1,0:T(8,128)(2,1)}), bf16[8192,512]{1,0:T(8,128)(2,1)}) %all-gather.3.cloned.1.call-update) | async-done | bytes 8388624 | tf_op jit(solution)/shard_map/all_gather | solution.py:350
  111.0 8.2 %shard_map.147 = (f32[4,256,512]{2,1,0:T(8,128)}, bf16[256,2048]{1,0:T(8,128)(2,1)}) custom-call(bf16[256,2048]{1,0:T(8,128)(2,1)} %shard_map.146.heads_ref, bf16[8,4,256,512]{3,2,1,0:T(8,128)(2,1)} %bitcast.77, bf16[256,2048]{1,0:T(8,128)(2,1)} %bitcast.82, f32[1,2048]{1,0:T(1,128)} %bitcast.85), custom_call_target="tpu_custom_call" | custom-call | flops 2147483648 | bytes 8388608 | tf_op jit(solution)/shard_map/pallas_call | solution.py:170
  119.2 2.5 convolution_convert_fusion
  121.7 111.2 %all_to_all.21 = bf16[8,128,2048]{2,1,0:T(8,128)(2,1)S(1)} all-to-all(bf16[8,128,2048]{2,1,0:T(8,128)(2,1)S(1)} %bitcast.76), channel_id=1, replica_groups=mesh['sp'=8,'dp'=4] {'sp'}, dimensions={0} | all-to-all | bytes 8388608 | tf_op jit(solution)/shard_map/all_to_all | solution.py:375
  233.0 4.5 %fusion.2 = f32[1024,1024]{1,0:T(8,128)S(1)} fusion(bf16[1024,2048]{1,0:T(8,128)(2,1)S(1)} %bitcast.79, bf16[1,2048,1024]{2,1,0:T(8,128)(2,1)S(1)} %copy-done.8), kind=kOutput, calls=%fused_computation.2 | convolution fusion | flops 4294967296 | bytes 12582912 | tf_op jit(solution)/shard_map/dot_general | solution.py:377
  237.5 5.4 %multiply_convert_fusion = bf16[1024,1024]{1,0:T(8,128)(2,1)S(1)} fusion(f32[1024,1024]{1,0:T(8,128)S(1)} %fusion.2, bf16[1024,2048]{1,0:T(8,128)(2,1)S(1)} %bitcast.80, bf16[1,2048,1024]{2,1,0:T(8,128)(2,1)S(1)} %copy-done.9), kind=kOutput, calls=%fused_computation.6 | convolution fusion | flops 4301258752 | bytes 14680064 | tf_op jit(solution)/shard_map/dot_general | solution.py:376
  242.9 6.1 %fusion.6 = bf16[1024,2048]{1,0:T(8,128)(2,1)} fusion(bf16[1024,1024]{1,0:T(8,128)(2,1)S(1)} %multiply_convert_fusion, bf16[1,1024,2048]{2,1,0:T(8,128)(2,1)S(1)} %copy-done.10), kind=kOutput, calls=%fused_computation.8 | convolution fusion | flops 4297064448 | bytes 10485760 | tf_op jit(solution)/shard_map/dot_general | solution.py:379
  249.0 4.7 %all-to-all-start.1 = ((bf16[8,128,2048]{2,1,0:T(8,128)(2,1)}), bf16[8,128,2048]{2,1,0:T(8,128)(2,1)}, u32[]{:S(2)}, u32[]{:S(2)}) async-start(bf16[8,128,2048]{2,1,0:T(8,128)(2,1)} %bitcast.78), calls=%async_computation.1 | async-start | bytes 8388608 | tf_op jit(solution)/shard_map/all_to_all | solution.py:382
  253.7 1.3 slice_bitcast_fusion.3
  255.0 91.7 %all-to-all-done.1 = bf16[8,128,2048]{2,1,0:T(8,128)(2,1)} async-done(((bf16[8,128,2048]{2,1,0:T(8,128)(2,1)}), bf16[8,128,2048]{2,1,0:T(8,128)(2,1)}, u32[]{:S(2)}, u32[]{:S(2)}) %all-to-all-start.1) | async-done | bytes 4194336 | tf_op jit(solution)/shard_map/all_to_all | solution.py:382
  346.6 3.5 convolution_bitcast_fusion
  350.2 4.5 %fusion.14 = bf16[1,256,2048]{2,1,0:T(8,128)(2,1)} fusion(f32[256,2048]{1,0:T(8,128)S(1)} %convolution_bitcast_fusion, bf16[8,128,2048]{2,1,0:T(8,128)(2,1)} %all-to-all-done.1, f32[256,512]{1,0:T(8,128)S(1)} %get-tuple-element.14, f32[256,512]{1,0:T(8,128)S(1)} %copy-done.1, f32[256,512]{1,0:T(8,128)S(1)} %copy-done.2, ...), kind=kOutput, calls=%fused_computation.14 | convolution fusion | flops 1078198272 | bytes 9455616 | tf_op jit(solution)/shard_map/dot_general | solution.py:385
  (43 shorter events, 1.2 us)
Async XLA Ops:
  6.5 7.5 %copy-start.4 = (bf16[1,256,256]{2,1,0:T(8,128)(2,1)S(1)}, bf16[1,256,256]{2,1,0:T(8,128)(2,1)}, u32[]{:S(2)}) copy-start(bf16[1,256,256]{2,1,0:T(8,128)(2,1)} %param.17) | copy-start | bytes 393220
  6.5 7.6 %copy-start.7 = (f32[256]{0:T(256)S(1)}, f32[256]{0:T(256)}, u32[]{:S(2)}) copy-start(f32[256]{0:T(256)} %param.20) | copy-start | bytes 3076
  6.5 8.5 %copy-start.3 = (bf16[1,256,16,64]{1,3,2,0:T(8,128)(2,1)S(1)}, bf16[1,256,16,64]{1,3,2,0:T(8,128)(2,1)}, u32[]{:S(2)}) copy-start(bf16[1,256,16,64]{1,3,2,0:T(8,128)(2,1)} %param.16) | copy-start | bytes 1572868
  6.5 104.4 %all-gather.3.cloned.1.call-start = ((), (), s32[]{:S(2)}) async-start(), calls=%async_computation.2 | async-start | bytes 8650752 | tf_op jit(solution)/shard_map/all_gather | solution.py:350
  121.7 111.3 %copy-start.8 = (bf16[1,2048,1024]{2,1,0:T(8,128)(2,1)S(1)}, bf16[1,2048,1024]{2,1,0:T(8,128)(2,1)}, u32[]{:S(2)}) copy-start(bf16[1,2048,1024]{2,1,0:T(8,128)(2,1)} %param.26) | copy-start | bytes 12582916
  233.0 4.5 %copy-start.9 = (bf16[1,2048,1024]{2,1,0:T(8,128)(2,1)S(1)}, bf16[1,2048,1024]{2,1,0:T(8,128)(2,1)}, u32[]{:S(2)}) copy-start(bf16[1,2048,1024]{2,1,0:T(8,128)(2,1)} %param.25) | copy-start | bytes 12582916
  237.5 5.4 %copy-start.10 = (bf16[1,1024,2048]{2,1,0:T(8,128)(2,1)S(1)}, bf16[1,1024,2048]{2,1,0:T(8,128)(2,1)}, u32[]{:S(2)}) copy-start(bf16[1,1024,2048]{2,1,0:T(8,128)(2,1)} %param.27) | copy-start | bytes 12582916
  249.0 4.7 %copy-start.5 = (s32[1,256,2]{1,2,0:T(2,128)S(1)}, s32[1,256,2]{1,2,0:T(2,128)}, u32[]{:S(2)}) copy-start(s32[1,256,2]{1,2,0:T(2,128)} %param.28) | copy-start | bytes 6148
  249.0 4.7 %copy-start.6 = (f32[1,256,2]{1,2,0:T(2,128)S(1)}, f32[1,256,2]{1,2,0:T(2,128)}, u32[]{:S(2)}) copy-start(f32[1,256,2]{1,2,0:T(2,128)} %param.29) | copy-start | bytes 6148
  249.0 4.7 %copy-start = (f32[4,256,512]{2,1,0:T(8,128)S(1)}, f32[4,256,512]{2,1,0:T(8,128)}, u32[]{:S(2)}) copy-start(f32[4,256,512]{2,1,0:T(8,128)} %get-tuple-element.11) | copy-start | bytes 6291460
  249.0 97.7 %all-to-all-start.1 = ((bf16[8,128,2048]{2,1,0:T(8,128)(2,1)}), bf16[8,128,2048]{2,1,0:T(8,128)(2,1)}, u32[]{:S(2)}, u32[]{:S(2)}) async-start(bf16[8,128,2048]{2,1,0:T(8,128)(2,1)} %bitcast.78), calls=%async_computation.1 | async-start | bytes 8388608 | tf_op jit(solution)/shard_map/all_to_all | solution.py:382
  254.9 95.2 %copy-start.1 = (f32[256,512]{1,0:T(8,128)S(1)}, f32[256,512]{1,0:T(8,128)}, u32[]{:S(2)}) copy-start(f32[256,512]{1,0:T(8,128)} %get-tuple-element.15) | copy-start | bytes 1572868
  254.9 95.2 %copy-start.2 = (f32[256,512]{1,0:T(8,128)S(1)}, f32[256,512]{1,0:T(8,128)}, u32[]{:S(2)}) copy-start(f32[256,512]{1,0:T(8,128)} %get-tuple-element.16) | copy-start | bytes 1572868
Sparse Core Ops, SparseCore 0:
  10.2 100.7 all-gather.2
